TPU v7x, 128 devices: a whole 4x4x4 slice. The times are simulated.
128 devices in a mesh: rep: 2 (over z_hi), fs: 32 (over z_lo, y, x), tp: 2 (over core).
Axes of the slice: x: 4, y: 4, z: 4 (z_hi: 2, z_lo: 2; z = z_hi * 2 + z_lo), core: 2. Of those that a mesh axis runs over, the one named last changes fastest.
Arguments:
- tokens: bfloat16 [65536, 2048], P(('rep', 'fs'), 'tp'), may hold values from -6 to 6
- attention_pre_gain: float32 [2048], replicated, may hold values from 0.1 to 1.9
- query_matrix: bfloat16 [2048, 512], P('fs', 'tp'), may hold values from -0.125 to 0.125
- key_matrix: bfloat16 [2048, 512], P('fs', 'tp'), may hold values from -0.125 to 0.125
- value_matrix: bfloat16 [2048, 1024], P('fs', 'tp'), may hold values from -0.125 to 0.125
- decay_first_weight: bfloat16 [2048, 16], replicated, may hold values from -0.125 to 0.125
- decay_second_weight: bfloat16 [16, 512], P(None, 'tp'), may hold values from -1.5 to 1.5
- decay_offset_bias: float32 [512], P('tp'), may hold values from 0 to 6
- extra_log_surge: float32 [65536, 2], P(('rep', 'fs'), 'tp'), may hold values from -0.7 to 0
- readout_head_gain: float32 [512], replicated, may hold values from 0.1 to 1.9
- output_matrix: bfloat16 [1024, 2048], P('tp', 'fs'), may hold values from -2.4375 to 2.4375
- attention_post_gain: float32 [2048], P('tp'), may hold values from 0.1 to 1.9
- feedforward_pre_gain: float32 [2048], replicated, may hold values from 0.1 to 1.9
- up_matrix: bfloat16 [2048, 4096], P('fs', 'tp'), may hold values from -0.125 to 0.125
- down_matrix: bfloat16 [4096, 2048], P('tp', 'fs'), may hold values from -1.21875 to 1.21875
- feedforward_post_gain: float32 [2048], P('tp'), may hold values from 0.1 to 1.9
Outputs:
- layer_out: bfloat16 [65536, 2048], P(('rep', 'fs'), 'tp')
All inputs are finite; a program needn't handle non-finite values.
Results may differ from a plain program's by a relative error of at most 0.017.
Values may be sent and summed in bfloat16 or wider, within the bound.
No kernel may reach another device: no remote copies, remote signals or barrier semaphores. Data moves between devices by JAX's collectives and lax.ppermute only.
A program may use at most 128 MiB of HBM per device.

v0:
```python
import jax
import jax.numpy as jnp
from jax import lax
from jax.sharding import Mesh
from jax.sharding import PartitionSpec as P

KEY_WIDTH = 256
DV = 512
BLOCK = 64
FS = ("fs_0", "fs_1", "fs_2")
REP_FS = ("rep", "fs_0", "fs_1", "fs_2")
EPS = 1e-06


def sent_together(arrays, axis, dim, along):
    both = jnp.concatenate(arrays, axis=along)
    filled, at, done = (lax.all_gather(both, axis, axis=dim, tiled=True), 0, [])
    for a in arrays:
        done.append(lax.slice_in_dim(filled, at, at + a.shape[along], axis=along))
        at += a.shape[along]
    return tuple(done)


def cut_along(array, dim, devices):
    lengths = array.shape
    tiles = array.reshape(*lengths[:dim], devices, lengths[dim] // devices, *lengths[dim + 1 :])
    return jnp.moveaxis(tiles, dim, 0)


def sum_at_owner(array, axis, dim):
    devices = lax.axis_size(axis)
    tiles = lax.all_to_all(cut_along(array, dim, devices), axis, 0, 0, tiled=True)
    return jnp.sum(tiles.astype(jnp.float32), axis=0)


def sent_to_all(array, axis):
    devices = lax.axis_size(axis)
    return lax.all_to_all(
        jnp.broadcast_to(array[None], (devices, *array.shape)), axis, 0, 0, tiled=True
    )


def taken_together(array, axis):
    everything = sent_to_all(array, axis)
    return jnp.sum(everything, axis=0)


def joined_along(tiles, dim):
    lengths = list(tiles.shape[1:])
    lengths[dim] *= tiles.shape[0]
    return jnp.moveaxis(tiles, 0, dim).reshape(lengths)


def stacked_from(array, axes, sequence):
    tiles = array
    for k in sequence:
        tiles = lax.all_gather(tiles, axes[k])
    done = sequence[::-1]
    back = [done.index(k) for k in range(len(axes))]
    tiles = tiles.transpose(*back, *range(len(axes), tiles.ndim))
    return tiles.reshape(-1, *array.shape)


def whole_of(array, axes, sequence, dim):
    return joined_along(stacked_from(array, axes, sequence), dim)


def pre_norm(rows, gain):
    values = rows.astype(jnp.float32)
    scale = lax.rsqrt(jnp.mean(values * values, axis=-1, keepdims=True) + EPS)
    return (values * scale * gain).astype(jnp.bfloat16)


def block_attention(queries, keys_in, values_in, log_gates):
    head_count, token_length, key_size = queries.shape
    value_size = values_in.shape[-1]
    blocks = token_length // BLOCK

    def to_blocks(array):
        return array.reshape(head_count, blocks, BLOCK, array.shape[-1]).transpose(1, 0, 2, 3)

    causal = jnp.tril(jnp.ones((BLOCK, BLOCK), dtype=bool))[None, :, :, None]
    highest = lax.Precision.HIGHEST

    def advance(memory_state, inputs):
        query_blk, key_blk, value_blk, gate_blk = inputs
        cumulative = jnp.cumsum(gate_blk, axis=1)
        carried = jnp.einsum(
            "hid,hde->hie", query_blk * jnp.exp(cumulative), memory_state, precision=highest
        )
        spread_log = cumulative[:, :, None, :] - cumulative[:, None, :, :]
        weights = jnp.exp(jnp.where(causal, spread_log, -jnp.inf))
        scores = jnp.einsum("hid,hjd,hijd->hij", query_blk, key_blk, weights, precision=highest)
        readout = carried + jnp.einsum("hij,hje->hie", scores, value_blk, precision=highest)
        final_log = cumulative[:, -1:, :]
        memory_state = jnp.exp(final_log[:, 0, :])[:, :, None] * memory_state + jnp.einsum(
            "hjd,hje->hde", key_blk * jnp.exp(final_log - cumulative), value_blk, precision=highest
        )
        return (memory_state, readout)

    start_state = jnp.zeros((head_count, key_size, value_size), jnp.float32)
    _, readout = lax.scan(
        advance,
        start_state,
        (to_blocks(queries), to_blocks(keys_in), to_blocks(values_in), to_blocks(log_gates)),
    )
    return readout.transpose(1, 0, 2, 3).reshape(head_count, token_length, value_size)


def make_adder(left):

    def add_rows(total, piece, start):
        return jnp.dot(left, piece, preferred_element_type=jnp.float32)

    return add_rows


def make_projector(left, piece):
    return jnp.dot(left, piece, preferred_element_type=jnp.float32)


def on_device(
    tokens,
    attention_pre_gain,
    query_matrix,
    key_matrix,
    value_matrix,
    decay_first_weight,
    decay_second_weight,
    decay_offset_bias,
    extra_log_surge,
    readout_head_gain,
    output_matrix,
    attention_post_gain,
    feedforward_pre_gain,
    up_matrix,
    down_matrix,
    feedforward_post_gain,
):
    token_length = tokens.shape[0]
    gathered = lax.all_gather(tokens, "tp", axis=1, tiled=True)
    width = gathered.shape[1]
    normed = pre_norm(gathered, attention_pre_gain)
    add_rows = make_adder(normed)
    key_cols = query_matrix.shape[1]
    value_cols = value_matrix.shape[1]
    empty_key = jnp.zeros((token_length, key_cols), jnp.float32)
    empty_value = jnp.zeros((token_length, value_cols), jnp.float32)
    pieces = sent_together((query_matrix, key_matrix, value_matrix), FS, 0, 1)
    start = jnp.int32(0)
    query_proj = add_rows(empty_key, pieces[0], start)
    key_proj = add_rows(empty_key, pieces[1], start)
    value_proj = add_rows(empty_value, pieces[2], start)
    query_proj = query_proj.astype(jnp.bfloat16)
    key_proj = key_proj.astype(jnp.bfloat16)
    value_proj = value_proj.astype(jnp.bfloat16)
    rank_rows = jnp.dot(normed, decay_first_weight, preferred_element_type=jnp.float32).astype(
        jnp.bfloat16
    )
    gate_source_input = (
        jnp.dot(rank_rows, decay_second_weight, preferred_element_type=jnp.float32)
        + decay_offset_bias
    )
    head_count = key_cols // KEY_WIDTH
    logarithm_decay = (jax.nn.log_sigmoid(gate_source_input) / 16.0).reshape(
        token_length, head_count, KEY_WIDTH
    ) + extra_log_surge[:, :, None]

    def by_head(array, size):
        return array.astype(jnp.float32).reshape(token_length, head_count, size).transpose(1, 0, 2)

    queries = by_head(query_proj, KEY_WIDTH) * KEY_WIDTH ** (-0.5)
    readout = block_attention(
        queries,
        by_head(key_proj, KEY_WIDTH),
        by_head(value_proj, DV),
        logarithm_decay.transpose(1, 0, 2),
    )
    readout = readout.transpose(1, 0, 2)
    head_scale = lax.rsqrt(jnp.mean(readout * readout, axis=-1, keepdims=True) + EPS)
    mixed = (
        (readout * head_scale * readout_head_gain)
        .astype(jnp.bfloat16)
        .reshape(token_length, value_cols)
    )
    partial_attn = make_projector(mixed, lax.all_gather(output_matrix, FS, axis=1, tiled=True))
    attn = sum_at_owner(partial_attn.astype(jnp.bfloat16), "tp", 1)
    attn_total = taken_together(jnp.sum(attn * attn, axis=1), "tp")
    attn_scale = lax.rsqrt(attn_total / width + EPS)[:, None]
    resid = (tokens.astype(jnp.float32) + attn * attn_scale * attention_post_gain).astype(
        jnp.bfloat16
    )
    gathered_mid = lax.all_gather(resid, "tp", axis=1, tiled=True)
    normed_mid = pre_norm(gathered_mid, feedforward_pre_gain)
    whole_up = whole_of(up_matrix, FS, (0, 1, 2), 0)
    hidden = jnp.dot(normed_mid, whole_up, preferred_element_type=jnp.float32)
    hidden = jax.nn.relu(hidden)
    squared = (hidden * hidden).astype(jnp.bfloat16)
    partial_feed = make_projector(squared, lax.all_gather(down_matrix, FS, axis=1, tiled=True))
    feed = sum_at_owner(partial_feed.astype(jnp.bfloat16), "tp", 1)
    feed_total = taken_together(jnp.sum(feed * feed, axis=1), "tp")
    feed_scale = lax.rsqrt(feed_total / width + EPS)[:, None]
    return (resid.astype(jnp.float32) + feed * feed_scale * feedforward_post_gain).astype(
        jnp.bfloat16
    )


def solution(mesh):
    finer = Mesh(
        mesh.devices.reshape(mesh.shape["rep"], 2, 4, 4, mesh.shape["tp"]),
        ("rep", "fs_0", "fs_1", "fs_2", "tp"),
    )
    in_specs = (
        P(REP_FS, "tp"),
        P(),
        P(FS, "tp"),
        P(FS, "tp"),
        P(FS, "tp"),
        P(),
        P(None, "tp"),
        P("tp"),
        P(REP_FS, "tp"),
        P(),
        P("tp", FS),
        P("tp"),
        P(),
        P(FS, "tp"),
        P("tp", FS),
        P("tp"),
    )
    out_specs = P(REP_FS, "tp")
    return jax.shard_map(
        on_device, mesh=finer, in_specs=in_specs, out_specs=out_specs, check_vma=False
    )
```

profile of v0, /device:TPU:1, one launch (start us, length us, event | category | flops | bytes accessed | tf_op | source)
XLA Modules:
  0.0 702.0 jit_solution(12112254873719032597)
XLA Ops:
  9.6 11.1 %all-gather = bf16[128,2048]{1,0:T(8,128)(2,1)} all-gather(bf16[64,2048]{1,0:T(8,128)(2,1)} %param.31), channel_id=2, replica_groups=mesh['rep'=2,'fs_0'=2,'fs_1'=4,'fs_2'=4,'tp'=2] {'fs_0'}, dimensions={0}, use_global_device_ids=true | all-gather | bytes 786432 | tf_op jit(solution)/shard_map/all_gather | solution.py:57
  20.8 8.2 %all-gather.11.cloned.1.call-done = bf16[1024,2048]{1,0:T(8,128)(2,1)} async-done(((bf16[1024,1024]{1,0:T(8,128)(2,1)}), bf16[1024,2048]{1,0:T(8,128)(2,1)}) %all-gather.11.cloned.1.call-update) | async-done | bytes 4194320 | tf_op jit(solution)/shard_map/all_gather | solution.py:141
  29.0 3.2 fusion.30
  32.5 3.0 fusion.32
  35.5 5.2 fusion.60
  40.7 127.3 %all-gather.13.cloned.1.call-done = bf16[2048,1024]{1,0:T(8,128)(2,1)} async-done(((bf16[64,1024]{1,0:T(8,128)(2,1)}), bf16[2048,1024]{1,0:T(8,128)(2,1)}) %all-gather.13.cloned.1.call-update) | async-done | bytes 4194320 | tf_op jit(solution)/shard_map/all_gather | solution.py:17
  168.0 5.3 fusion.52
  177.3 2.3 fusion.57
  179.6 150.9 %while.13 = (s32[]{:T(128)}, f32[1,256,512]{2,1,0:T(8,128)S(1)}, f32[16,1,64,512]{3,2,1,0:T(8,128)S(1)}, f32[16,1,64,256]{3,2,1,0:T(8,128)}, f32[16,1,64,256]{3,...) while((s32[]{:T(128)}, f32[1,256,512]{2,1,0:T(8,128)S(1)}, ...), condition=%wide.region_3.4_spmd.clone, body=%wide.region_1.3_spmd.clone.sunk | while | flops 233373696 | bytes 11649660 | solution.py:102
  182.3 2.5 fusion.94
  187.3 1.6 fusion.92
  191.7 2.5 fusion.94
  196.8 1.6 fusion.92
  201.1 2.5 fusion.94
  206.2 1.6 fusion.92
  210.6 2.5 fusion.94
  220.0 2.5 fusion.94
  225.1 1.6 fusion.92
  229.4 2.5 fusion.94
  238.9 2.5 fusion.94
  243.9 1.6 fusion.92
  248.3 2.5 fusion.94
  253.4 1.6 fusion.92
  257.7 2.5 fusion.94
  267.2 2.5 fusion.94
  276.6 2.5 fusion.94
  286.0 2.5 fusion.94
  295.5 2.5 fusion.94
  304.9 2.5 fusion.94
  314.3 2.5 fusion.94
  323.7 2.5 fusion.94
  328.8 1.6 fusion.92
  332.0 4.3 convolution_convert_fusion
  336.8 27.5 %all_to_all.22 = bf16[2,1024,1024]{2,1,0:T(8,128)(2,1)S(1)} all-to-all(bf16[2,1024,1024]{2,1,0:T(8,128)(2,1)S(1)} %bitcast.148), channel_id=1, replica_groups=mesh['rep'=2,'fs_0'=2,'fs_1'=4,'fs_2'=4,'tp'=2] {'tp'}, dimensions={0} | all-to-all | bytes 8388608 | tf_op jit(solution)/shard_map/all_to_all | solution.py:32
  365.4 1.9 copy-done.3
  367.7 3.9 all_to_all.23
  371.6 4.2 add_convert_fusion.1
  377.2 16.5 %all-gather.17.cloned.1.call-done = bf16[1024,2048]{1,0:T(8,128)(2,1)} async-done(((bf16[1024,1024]{1,0:T(8,128)(2,1)}), bf16[1024,2048]{1,0:T(8,128)(2,1)}) %all-gather.17.cloned.1.call-update) | async-done | bytes 4194320 | tf_op jit(solution)/shard_map/all_gather | solution.py:193
  393.7 3.1 fusion.33
  396.8 82.2 %all-gather.23.cloned.1.call-done = bf16[16,2,64,2048]{3,2,1,0:T(8,128)(2,1)} async-done(((bf16[4,2,64,2048]{3,2,1,0:T(8,128)(2,1)}), bf16[16,2,64,2048]{3,2,1,0:T(8,128)(2,1)}) %all-gather.23.cloned.1.call-update) | async-done | bytes 8388624 | tf_op jit(solution)/shard_map/all_gather | solution.py:57
  479.0 8.3 %copy.56 = bf16[2,4,4,64,2048]{4,3,2,1,0:T(8,128)(2,1)} copy(bf16[2,4,4,64,2048]{4,3,0,1,2:T(8,128)(2,1)} %bitcast.150) | data formatting | bytes 16777216 | tf_op jit(solution)/shard_map/transpose | solution.py:60
  487.3 140.4 %all-gather.19.cloned.1.call-done = bf16[2048,2048]{0,1:T(8,128)(2,1)} async-done(((bf16[2048,64]{0,1:T(8,128)(2,1)}), bf16[2048,2048]{0,1:T(8,128)(2,1)}) %all-gather.19.cloned.1.call-update) | async-done | bytes 8388624 | tf_op jit(solution)/shard_map/all_gather | solution.py:199
  627.7 25.6 %fusion.45 = bf16[1024,2048]{1,0:T(8,128)(2,1)} fusion(bf16[2048,2048]{0,1:T(8,128)(2,1)} %all-gather.19.cloned.1.call-done, bf16[2048,2048]{1,0:T(8,128)(2,1)} %bitcast.151, bf16[1024,2048]{1,0:T(8,128)(2,1)} %all-gather.17.cloned.1.call-done, f32[2048]{0:T(1024)S(1)} %copy-done.14, f32[1024]{0:T(1024)S(1)} %add_rsqrt_fusion.2), kind=kOutput, calls=%fused_computation.61 | convolution fusion | flops 17196646400 | bytes 25178112 | tf_op jit(solution)/shard_map/dot_general | solution.py:119
  653.3 2.6 copy.73
  655.9 27.7 %all_to_all.24 = bf16[2,1024,1024]{2,1,0:T(8,128)(2,1)S(1)} all-to-all(bf16[2,1024,1024]{2,1,0:T(8,128)(2,1)S(1)} %bitcast.149), channel_id=1, replica_groups=mesh['rep'=2,'fs_0'=2,'fs_1'=4,'fs_2'=4,'tp'=2] {'tp'}, dimensions={0} | all-to-all | bytes 8388608 | tf_op jit(solution)/shard_map/all_to_all | solution.py:32
  684.7 1.9 copy-done.2
  687.0 3.9 all_to_all.25
  690.9 4.2 add_convert_fusion
  (224 shorter events, 111.7 us)
Async XLA Ops:
  6.5 29.0 %copy-start = (bf16[2048,16]{0,1:T(8,128)(2,1)S(1)}, bf16[2048,16]{0,1:T(8,128)(2,1)}, u32[]{:S(2)}) copy-start(bf16[2048,16]{0,1:T(8,128)(2,1)} %param.23) | copy-start | bytes 196612
  6.5 25.7 %copy-start.8 = (f32[2048]{0:T(1024)S(1)}, f32[2048]{0:T(1024)}, u32[]{:S(2)}) copy-start(f32[2048]{0:T(1024)} %param.19) | copy-start | bytes 24580
  6.5 22.5 %all-gather.11.cloned.1.call-start = ((), (), s32[]{:S(2)}) async-start(), calls=%async_computation.4 | async-start | bytes 6291456 | tf_op jit(solution)/shard_map/all_gather | solution.py:141
  7.3 160.7 %all-gather.13.cloned.1.call-start = ((), (), s32[]{:S(2)}) async-start(), calls=%async_computation.5 | async-start | bytes 4325376 | tf_op jit(solution)/shard_map/all_gather | solution.py:17
  8.8 323.2 %all-gather.15.cloned.1.call-start = ((), (), s32[]{:S(2)}) async-start(), calls=%async_computation.6 | async-start | bytes 2162688 | tf_op jit(solution)/shard_map/all_gather | solution.py:186
  9.6 366.3 %all-gather.21.cloned.1.call-start = ((), (), s32[]{:S(2)}) async-start(), calls=%async_computation.9 | async-start | bytes 2621440 | tf_op jit(solution)/shard_map/all_gather | solution.py:57
  20.7 372.9 %all-gather.17.cloned.1.call-start = ((), (), s32[]{:S(2)}) async-start(), calls=%async_computation.7 | async-start | bytes 6291456 | tf_op jit(solution)/shard_map/all_gather | solution.py:193
  29.0 3.4 copy-start.5
  32.5 3.0 copy-start.13
  32.5 3.0 copy-start.15
  32.5 3.0 copy-start.16
  168.0 6.9 copy-start.7
  168.0 6.9 copy-start.12
  179.6 151.2 %copy-start.11 = (f32[512]{0:T(512)S(1)}, f32[512]{0:T(512)}, u32[]{:S(2)}) copy-start(f32[512]{0:T(512)} %param.27) | copy-start | bytes 6148
  365.4 1.9 copy-start.3
  367.3 4.3 copy-start.6
  367.3 4.3 copy-start.9
  375.8 103.2 %all-gather.23.cloned.1.call-start = ((), (), s32[]{:S(2)}) async-start(), calls=%async_computation.10 | async-start | bytes 10485760 | tf_op jit(solution)/shard_map/all_gather | solution.py:57
  376.4 251.3 %all-gather.19.cloned.1.call-start = ((), (), s32[]{:S(2)}) async-start(), calls=%async_computation.8 | async-start | bytes 8650752 | tf_op jit(solution)/shard_map/all_gather | solution.py:199
  479.0 148.7 %copy-start.14 = (f32[2048]{0:T(1024)S(1)}, f32[2048]{0:T(1024)}, u32[]{:S(2)}) copy-start(f32[2048]{0:T(1024)} %param.30) | copy-start | bytes 24580
  684.7 1.9 copy-start.2
  686.6 4.3 copy-start.4
  686.6 4.3 copy-start.10
  690.9 4.2 copy-start.1
Sparse Core Ops, SparseCore 0:
  9.0 19.9 all-gather.10
  30.7 137.2 all-gather.12
  169.6 151.2 all-gather.14
  322.4 52.6 all-gather.20
  376.7 16.9 all-gather.16
  395.2 83.7 all-gather.22
  480.7 147.0 all-gather.18
where the time goes:
time: 705 us; the launch traced here: 702 us
  waiting for transfers between devices  377 us (53%)
  matrix products  111 us (16%)
  other arithmetic  81.5 us (12%)
  blocking collectives  74 us (10%)
  local copies, waits for them, and re-layouts  43.6 us (6%)
  between operations  13.7 us (2%)
    all_gather x1, waiting for transfers between devices, on_device(): lax.all_gather(down_matrix, FS, axis=1, tiled=True)  140 us
    all_gather x1, waiting for transfers between devices, sent_together(): filled, at, done = (lax.all_gather(both, axis, axis=dim, tiled=True), 0, [])  127 us
    all_gather x2, waiting for transfers between devices, stacked_from(): tiles = lax.all_gather(tiles, axes[k])  82.3 us
    all_to_all x2, blocking collectives, sum_at_owner(): lax.all_to_all(cut_along(array, dim, devices), axis, 0, 0, tiled=True)  55.2 us
    dot_general x16, other arithmetic, advance(): jnp.einsum('hid,hjd,hijd->hij', query_blk, key_blk, weights, precision=hi...  40.2 us
    dot_general x2, matrix products, make_projector(): return jnp.dot(left, piece, preferred_element_type=jnp.float32)  29.9 us
    dot_general x16, matrix products, advance(): jnp.einsum('hjd,hje->hde', key_blk * jnp.exp(final_log - cumulative), val...  26.2 us
    dot_general x16, matrix products, advance(): jnp.einsum('hid,hde->hie', query_blk * jnp.exp(cumulative), memory_state,...  20.8 us
  transfers between devices with their start and end apart: 7, of which 5 were waited for; matrix products, arithmetic and copies ran while one was open for 28% of the time, Pallas kernels for 0%

commit v1 on v0

--- a/solution.py
+++ b/solution.py
@@ -10,6 +10,13 @@
 FS = ("fs_0", "fs_1", "fs_2")
 REP_FS = ("rep", "fs_0", "fs_1", "fs_2")
 EPS = 1e-06
+
+
+def all_by_exchange(x, axis, along):
+    size = lax.axis_size(axis)
+    tiles = jnp.stack([x for _ in range(size)])
+    tiles = lax.all_to_all(tiles, axis, split_axis=0, concat_axis=0)
+    return jnp.concatenate(tiles, axis=along)
 
 
 def sent_together(arrays, axis, dim, along):
@@ -196,7 +203,7 @@
     hidden = jnp.dot(normed_mid, whole_up, preferred_element_type=jnp.float32)
     hidden = jax.nn.relu(hidden)
     squared = (hidden * hidden).astype(jnp.bfloat16)
-    partial_feed = make_projector(squared, lax.all_gather(down_matrix, FS, axis=1, tiled=True))
+    partial_feed = make_projector(squared, all_by_exchange(down_matrix, FS, 1))
     feed = sum_at_owner(partial_feed.astype(jnp.bfloat16), "tp", 1)
     feed_total = taken_together(jnp.sum(feed * feed, axis=1), "tp")
     feed_scale = lax.rsqrt(feed_total / width + EPS)[:, None]

time: 705 us -> 617 us (0.88)
  waiting for transfers between devices: 377 us -> 299 us
  blocking collectives: 74 us -> 53.4 us
    all_gather x1 -> x0, waiting for transfers between devices: 140 us -> none  [on_device(): lax.all_gather(down_matrix, FS, axis=1, tiled=True)]
    all_gather x2, waiting for transfers between devices: 82.3 us -> 155 us  [stacked_from(): tiles = lax.all_gather(tiles, axes[k])]
    all_to_all x2, blocking collectives: 55.2 us -> 34.6 us  [sum_at_owner(): lax.all_to_all(cut_along(array, dim, devices), axis, 0, 0, tiled=True)]
    all_gather x1, waiting for transfers between devices: 16.5 us -> 7.28 us  [on_device(): gathered_mid = lax.all_gather(resid, 'tp', axis=1, tiled=True)]
    another operation x16 -> x17, local copies, waits for them, and re-layouts: 14.2 us -> 18.5 us
  transfers between devices with their start and end apart: 7 -> 7, of which waited for: 5 -> 5; matrix products, arithmetic and copies ran while one was open for 28% -> 33% of each run, Pallas kernels for 0% -> 0%
where the time goes in v1:
time: 617 us; the launch traced here: 612 us
  waiting for transfers between devices  299 us (48%)
  matrix products  110 us (18%)
  other arithmetic  79.8 us (13%)
  blocking collectives  53.4 us (9%)
  local copies, waits for them, and re-layouts  48.1 us (8%)
  between operations  13.7 us (2%)
  starting transfers between devices  7.1 us (1%)
    all_gather x2, waiting for transfers between devices, stacked_from(): tiles = lax.all_gather(tiles, axes[k])  155 us
    all_gather x1, waiting for transfers between devices, sent_together(): filled, at, done = (lax.all_gather(both, axis, axis=dim, tiled=True), 0, [])  127 us
    dot_general x16, other arithmetic, advance(): jnp.einsum('hid,hjd,hijd->hij', query_blk, key_blk, weights, precision=hi...  38.5 us
    all_to_all x2, blocking collectives, sum_at_owner(): lax.all_to_all(cut_along(array, dim, devices), axis, 0, 0, tiled=True)  34.6 us
    dot_general x2, matrix products, make_projector(): return jnp.dot(left, piece, preferred_element_type=jnp.float32)  29.9 us
    dot_general x16, matrix products, advance(): jnp.einsum('hjd,hje->hde', key_blk * jnp.exp(final_log - cumulative), val...  26.2 us
    dot_general x16, matrix products, advance(): jnp.einsum('hid,hde->hie', query_blk * jnp.exp(cumulative), memory_state,...  20.8 us
    dot_general x16, matrix products, advance(): jnp.einsum('hij,hje->hie', scores, value_blk, precision=highest)  19.6 us
  transfers between devices with their start and end apart: 7, of which 5 were waited for; matrix products, arithmetic and copies ran while one was open for 33% of the time, Pallas kernels for 0%

profile of v1, /device:TPU:1, one launch (start us, length us, event | category | flops | bytes accessed | tf_op | source)
XLA Modules:
  0.0 612.0 jit_solution(17530343071921427471)
XLA Ops:
  9.6 11.1 %all-gather = bf16[128,2048]{1,0:T(8,128)(2,1)} all-gather(bf16[64,2048]{1,0:T(8,128)(2,1)} %param.31), channel_id=2, replica_groups=mesh['rep'=2,'fs_0'=2,'fs_1'=4,'fs_2'=4,'tp'=2] {'fs_0'}, dimensions={0}, use_global_device_ids=true | all-gather | bytes 786432 | tf_op jit(solution)/shard_map/all_gather | solution.py:64
  20.8 8.2 %all-gather.10.cloned.1.call-done = bf16[1024,2048]{1,0:T(8,128)(2,1)} async-done(((bf16[1024,1024]{1,0:T(8,128)(2,1)}), bf16[1024,2048]{1,0:T(8,128)(2,1)}) %all-gather.10.cloned.1.call-update) | async-done | bytes 4194320 | tf_op jit(solution)/shard_map/all_gather | solution.py:148
  29.0 3.2 fusion.30
  32.5 3.0 fusion.32
  35.5 5.2 fusion.60
  40.7 127.3 %all-gather.12.cloned.1.call-done = bf16[2048,1024]{1,0:T(8,128)(2,1)} async-done(((bf16[64,1024]{1,0:T(8,128)(2,1)}), bf16[2048,1024]{1,0:T(8,128)(2,1)}) %all-gather.12.cloned.1.call-update) | async-done | bytes 4194320 | tf_op jit(solution)/shard_map/all_gather | solution.py:24
  168.0 3.9 convolution_convert_fusion.2
  173.1 2.3 fusion.52
  177.1 2.2 fusion.57
  179.3 149.1 %while.13 = (s32[]{:T(128)}, f32[1,256,512]{2,1,0:T(8,128)S(1)}, f32[16,1,64,512]{3,2,1,0:T(8,128)S(1)}, f32[16,1,64,256]{3,2,1,0:T(8,128)}, f32[16,1,64,256]{3,...) while((s32[]{:T(128)}, f32[1,256,512]{2,1,0:T(8,128)S(1)}, ...), condition=%wide.region_3.4_spmd.clone, body=%wide.region_1.3_spmd.clone.sunk | while | flops 233373696 | bytes 11650182 | solution.py:109
  182.0 2.4 fusion.94
  191.3 2.4 fusion.94
  196.3 1.6 fusion.92
  200.6 2.4 fusion.94
  205.6 1.6 fusion.92
  210.0 2.4 fusion.94
  219.3 2.4 fusion.94
  228.6 2.4 fusion.94
  233.6 1.6 fusion.92
  237.9 2.4 fusion.94
  247.3 2.4 fusion.94
  256.6 2.4 fusion.94
  265.9 2.4 fusion.94
  270.8 1.6 fusion.92
  275.2 2.4 fusion.94
  280.2 1.6 fusion.92
  284.6 2.4 fusion.94
  293.9 2.4 fusion.94
  303.2 2.4 fusion.94
  312.5 2.4 fusion.94
  321.8 2.4 fusion.94
  330.0 4.3 convolution_convert_fusion
  334.8 27.4 %all_to_all.27 = bf16[2,1024,1024]{2,1,0:T(8,128)(2,1)S(1)} all-to-all(bf16[2,1024,1024]{2,1,0:T(8,128)(2,1)S(1)} %bitcast.151), channel_id=1, replica_groups=mesh['rep'=2,'fs_0'=2,'fs_1'=4,'fs_2'=4,'tp'=2] {'tp'}, dimensions={0} | all-to-all | bytes 8388608 | tf_op jit(solution)/shard_map/all_to_all | solution.py:39
  363.2 1.9 copy-done.3
  365.5 3.9 all_to_all.28
  369.4 4.2 add_convert_fusion.1
  375.2 4.3 stack.2
  379.5 6.9 %all-to-all-start.2 = ((bf16[32,2048,64]{1,2,0:T(8,128)(2,1)}), bf16[32,2048,64]{1,2,0:T(8,128)(2,1)}, u32[]{:S(2)}, u32[]{:S(2)}) async-start(bf16[32,2048,64]{1,2,0:T(8,128)(2,1)} %stack.2), calls=%async_computation.2 | async-start | bytes 16777216 | tf_op jit(solution)/shard_map/all_to_all | solution.py:18
  386.4 7.3 %all-gather.16.cloned.1.call-done = bf16[1024,2048]{1,0:T(8,128)(2,1)} async-done(((bf16[1024,1024]{1,0:T(8,128)(2,1)}), bf16[1024,2048]{1,0:T(8,128)(2,1)}) %all-gather.16.cloned.1.call-update) | async-done | bytes 4194320 | tf_op jit(solution)/shard_map/all_gather | solution.py:200
  393.7 3.1 fusion.33
  396.8 153.1 %all-gather.20.cloned.1.call-done = bf16[16,2,64,2048]{3,2,1,0:T(8,128)(2,1)} async-done(((bf16[4,2,64,2048]{3,2,1,0:T(8,128)(2,1)}), bf16[16,2,64,2048]{3,2,1,0:T(8,128)(2,1)}) %all-gather.20.cloned.1.call-update) | async-done | bytes 8388624 | tf_op jit(solution)/shard_map/all_gather | solution.py:64
  549.9 8.3 %copy.57 = bf16[2,4,4,64,2048]{4,3,2,1,0:T(8,128)(2,1)} copy(bf16[2,4,4,64,2048]{4,3,0,1,2:T(8,128)(2,1)} %bitcast.153) | data formatting | bytes 16777216 | tf_op jit(solution)/shard_map/transpose | solution.py:67
  558.2 25.6 %fusion.45 = bf16[1024,2048]{1,0:T(8,128)(2,1)} fusion(bf16[2048,2048]{0,1:T(8,128)(2,1)} %bitcast.18, bf16[2048,2048]{1,0:T(8,128)(2,1)} %bitcast.154, bf16[1024,2048]{1,0:T(8,128)(2,1)} %all-gather.16.cloned.1.call-done, f32[2048]{0:T(1024)S(1)} %copy-done.15, f32[1024]{0:T(1024)S(1)} %add_rsqrt_fusion.2), kind=kOutput, calls=%fused_computation.61 | convolution fusion | flops 17196646400 | bytes 25178112 | tf_op jit(solution)/shard_map/dot_general | solution.py:126
  583.8 2.6 copy.74
  586.4 7.2 %all_to_all.29 = bf16[2,1024,1024]{2,1,0:T(8,128)(2,1)S(1)} all-to-all(bf16[2,1024,1024]{2,1,0:T(8,128)(2,1)S(1)} %bitcast.152), channel_id=1, replica_groups=mesh['rep'=2,'fs_0'=2,'fs_1'=4,'fs_2'=4,'tp'=2] {'tp'}, dimensions={0} | all-to-all | bytes 8388608 | tf_op jit(solution)/shard_map/all_to_all | solution.py:39
  594.7 1.9 copy-done.2
  597.0 3.9 all_to_all.30
  601.0 4.2 add_convert_fusion
  (226 shorter events, 114.2 us)
Async XLA Ops:
  6.5 29.0 %copy-start = (bf16[2048,16]{0,1:T(8,128)(2,1)S(1)}, bf16[2048,16]{0,1:T(8,128)(2,1)}, u32[]{:S(2)}) copy-start(bf16[2048,16]{0,1:T(8,128)(2,1)} %param.23) | copy-start | bytes 196612
  6.5 25.7 %copy-start.9 = (f32[2048]{0:T(1024)S(1)}, f32[2048]{0:T(1024)}, u32[]{:S(2)}) copy-start(f32[2048]{0:T(1024)} %param.19) | copy-start | bytes 24580
  6.5 22.5 %all-gather.10.cloned.1.call-start = ((), (), s32[]{:S(2)}) async-start(), calls=%async_computation.5 | async-start | bytes 6291456 | tf_op jit(solution)/shard_map/all_gather | solution.py:148
  7.3 160.7 %all-gather.12.cloned.1.call-start = ((), (), s32[]{:S(2)}) async-start(), calls=%async_computation.6 | async-start | bytes 4325376 | tf_op jit(solution)/shard_map/all_gather | solution.py:24
  8.8 321.1 %all-gather.14.cloned.1.call-start = ((), (), s32[]{:S(2)}) async-start(), calls=%async_computation.7 | async-start | bytes 2162688 | tf_op jit(solution)/shard_map/all_gather | solution.py:193
  9.6 365.6 %all-gather.18.cloned.1.call-start = ((), (), s32[]{:S(2)}) async-start(), calls=%async_computation.9 | async-start | bytes 2621440 | tf_op jit(solution)/shard_map/all_gather | solution.py:64
  20.7 373.0 %all-gather.16.cloned.1.call-start = ((), (), s32[]{:S(2)}) async-start(), calls=%async_computation.8 | async-start | bytes 6291456 | tf_op jit(solution)/shard_map/all_gather | solution.py:200
  29.0 3.4 copy-start.5
  32.5 3.0 copy-start.14
  32.5 3.0 copy-start.16
  32.5 3.0 copy-start.17
  168.0 5.0 copy-start.7
  168.0 5.1 copy-start.13
  179.3 149.5 %copy-start.12 = (f32[512]{0:T(512)S(1)}, f32[512]{0:T(512)}, u32[]{:S(2)}) copy-start(f32[512]{0:T(512)} %param.27) | copy-start | bytes 6148
  363.2 1.9 copy-start.3
  365.1 4.3 copy-start.6
  365.1 4.3 copy-start.10
  373.7 1.6 copy-start.8
  373.7 176.2 %all-gather.20.cloned.1.call-start = ((), (), s32[]{:S(2)}) async-start(), calls=%async_computation.10 | async-start | bytes 10485760 | tf_op jit(solution)/shard_map/all_gather | solution.py:64
  379.5 178.7 %all-to-all-start.2 = ((bf16[32,2048,64]{1,2,0:T(8,128)(2,1)}), bf16[32,2048,64]{1,2,0:T(8,128)(2,1)}, u32[]{:S(2)}, u32[]{:S(2)}) async-start(bf16[32,2048,64]{1,2,0:T(8,128)(2,1)} %stack.2), calls=%async_computation.2 | async-start | bytes 16777216 | tf_op jit(solution)/shard_map/all_to_all | solution.py:18
  549.9 8.3 %copy-start.15 = (f32[2048]{0:T(1024)S(1)}, f32[2048]{0:T(1024)}, u32[]{:S(2)}) copy-start(f32[2048]{0:T(1024)} %param.30) | copy-start | bytes 24580
  594.7 1.9 copy-start.2
  596.7 4.3 copy-start.4
  596.7 4.3 copy-start.11
  600.9 4.2 copy-start.1
Sparse Core Ops, SparseCore 0:
  9.0 19.9 all-gather.9
  30.7 137.2 all-gather.11
  169.6 151.6 all-gather.13
  322.9 52.3 all-gather.17
  376.7 16.9 all-gather.15
  395.2 154.6 all-gather.19
